TPU v7x, 32 devices: a whole 2x2x4 slice. The times are simulated.
32 devices in a mesh: row: 4 (over y, x), col: 8 (over z, core).
Axes of the slice: x: 2, y: 2, z: 4, core: 2. Of those that a mesh axis runs over, the one named last changes fastest.
Arguments:
- mix_input: bfloat16 [4, 4096, 512], P(None, ('row', 'col')), may hold values from -6 to 6
- group_maps: bfloat16 [4, 128, 128], replicated, may hold values from -0.5 to 0.5
- out_map: bfloat16 [512, 2048], replicated, may hold values from -0.25 to 0.25
Outputs:
- mixed: bfloat16 [4, 4096, 2048], P(None, ('row', 'col'))
All inputs are finite; a program needn't handle non-finite values.
Results may differ from a plain program's by a relative error of at most 0.011.
Values may be sent and summed in bfloat16 or wider, within the bound.
A program may use at most 64 MiB of HBM per device.

v0:
```python
import math

import jax
import jax.numpy as jnp
import numpy as np
from jax import lax
from jax.experimental import pallas as pl
from jax.experimental.pallas import tpu as pltpu
from jax.sharding import PartitionSpec as P

AXES = ("row", "col")


def turn_tables(left_count, right_count, modulus):
    turns = np.arange(left_count)[:, None] * np.arange(right_count)[None, :] % modulus
    angles = turns * (2.0 * math.pi / modulus)
    return np.cos(angles), np.sin(angles)


def lane_tables(width):
    cosine, sine = turn_tables(width, width, width)
    half = width // 2
    pack = np.zeros((width, width))
    unpack = np.zeros((width, width))
    pack[:, 0::2] = cosine[:, :half]
    pack[:, 1::2] = -sine[:, :half]
    pack[:, 1] = cosine[:, half]
    unpack[0, 0] = 1.0
    unpack[1, half] = 1.0
    for freq in range(1, half):
        unpack[2 * freq, freq] = unpack[2 * freq, width - freq] = 1.0
        unpack[2 * freq + 1, freq] = 1.0
        unpack[2 * freq + 1, width - freq] = -1.0
    return pack, unpack


def fourier(values):
    count = len(values)
    if count == 1:
        return values
    even, odd = fourier(values[0::2]), fourier(values[1::2])
    low, high = [], []
    for at in range(count // 2):
        cosine = math.cos(2.0 * math.pi * at / count)
        sine = math.sin(2.0 * math.pi * at / count)
        (even_re, even_im), (odd_re, odd_im) = even[at], odd[at]
        if at == 0:
            turn_re, turn_im = odd_re, odd_im
        elif 4 * at == count:
            turn_re, turn_im = odd_im, -odd_re
        elif odd_im is None:
            turn_re, turn_im = odd_re * cosine, odd_re * -sine
        else:
            turn_re = odd_re * cosine + odd_im * sine
            turn_im = odd_im * cosine - odd_re * sine
        if turn_re is None:
            low_re = high_re = even_re
        else:
            low_re, high_re = even_re + turn_re, even_re - turn_re
        if turn_im is None:
            low_im = high_im = even_im
        elif even_im is None:
            low_im, high_im = turn_im, -turn_im
        else:
            low_im, high_im = even_im + turn_im, even_im - turn_im
        low.append((low_re, low_im))
        high.append((high_re, high_im))
    return low + high


def mixing_kernel(
    x_hbm, pack_hbm, cos_hbm, sin_hbm, table_hbm, unpack_hbm, given_hbm, out_ref,
    x_ref, pack_ref, cos_ref, sin_ref, table_ref, unpack_ref, given_ref, maps, load_sem,
    send, held, stack, big, send_back, back, send_sem, recv_sem, send_back_sem, recv_back_sem,
):
    bf16, f32 = jnp.bfloat16, jnp.float32
    seqs, positions, channels = x_ref.shape
    devices, items, _ = send.shape
    width = pack_ref.shape[0]
    groups = channels // width
    cols = lax.axis_size("col")
    me = lax.axis_index("row") * cols + lax.axis_index("col")
    far_refs = (x_hbm, pack_hbm, cos_hbm, sin_hbm, table_hbm, unpack_hbm, given_hbm)
    near_refs = (x_ref, pack_ref, cos_ref, sin_ref, table_ref, unpack_ref, given_ref)
    loads = [
        pltpu.make_async_copy(src, dst, load_sem.at[at])
        for at, (src, dst) in enumerate(zip(far_refs, near_refs))
    ]
    for load in loads:
        load.start()
    barrier = pltpu.get_barrier_semaphore()

    def peer_of(step):
        peer = lax.rem(me + step, devices)
        return peer, (lax.div(peer, cols), lax.rem(peer, cols))

    def greet(step, carry):
        pl.semaphore_signal(
            barrier, inc=1, device_id=peer_of(step)[1], device_id_type=pl.DeviceIdType.MESH
        )
        return carry

    lax.fori_loop(1, devices, greet, 0)
    rows_t = (((1,), (1,)), ((), ()))
    loads[0].wait()
    loads[1].wait()
    for s in range(seqs):
        for g in range(groups):
            lanes = lax.dot_general(
                pack_ref[...], x_ref[s, :, g * width : (g + 1) * width], rows_t,
                preferred_element_type=f32,
            ).astype(bf16)
            for half in range(2):
                send[(s * groups + g) * 2 + half] = lanes[half * items : (half + 1) * items]
    pl.semaphore_wait(barrier, devices - 1)

    def exchange(src, dst, out_sem, in_sem, beside):
        def copy(step):
            peer, where = peer_of(step)
            return pltpu.make_async_remote_copy(
                src_ref=src.at[peer], dst_ref=dst.at[me], send_sem=out_sem.at[peer],
                recv_sem=in_sem.at[me], device_id=where, device_id_type=pl.DeviceIdType.MESH,
            )

        def arrival(step):
            peer, where = peer_of(step)
            return pltpu.make_async_remote_copy(
                src_ref=src.at[peer], dst_ref=dst.at[peer], send_sem=out_sem.at[peer],
                recv_sem=in_sem.at[peer], device_id=where, device_id_type=pl.DeviceIdType.MESH,
            )

        def start(step, carry):
            copy(step).start()
            return carry

        def finish(step, carry):
            arrival(step).wait_recv()
            copy(step).wait_send()
            return carry

        lax.fori_loop(1, devices, start, 0)
        dst[me] = src[me]
        beside()
        lax.fori_loop(1, devices, finish, 0)

    def ready_maps():
        for load in loads[2:]:
            load.wait()
        for g in range(groups):
            maps[g] = jnp.dot(
                unpack_ref[...], given_ref[g], preferred_element_type=f32
            ).astype(bf16)

    exchange(send, held, send_sem, recv_sem, ready_maps)

    tile = 16
    def spin(chunk, carry):
        rows = pl.ds(pl.multiple_of(chunk * tile, tile), tile)
        spun = fourier([(held[d, rows, :].astype(f32), None) for d in range(devices)])
        row_ids = chunk * tile + lax.broadcasted_iota(jnp.int32, (tile, positions), 0)
        lane_ids = lax.rem(me * items + row_ids, width)
        is_sine = (lax.rem(lane_ids, 2) == 1) & (lane_ids != 1)
        for f in range(devices):
            real_in, imag_in = spun[f]
            cosine, sine = cos_ref[f : f + 1, :], sin_ref[f : f + 1, :]
            if imag_in is None:
                real_part, imag_part = real_in * cosine, -(real_in * sine)
            else:
                real_part = real_in * cosine + imag_in * sine
                imag_part = imag_in * cosine - real_in * sine
            stack[f, rows, :positions] = jnp.where(is_sine, -imag_part, real_part).astype(bf16)
            stack[f, rows, positions:] = jnp.where(is_sine, real_part, imag_part).astype(bf16)
        return carry

    lax.fori_loop(0, items // tile, spin, 0)
    pairs = devices // 2
    for a in range(pairs):
        both = jnp.concatenate([stack[a], stack[a + pairs]], axis=0)
        big[pl.ds(a, positions, stride=pairs), :] = lax.dot_general(
            table_ref[...], both, rows_t, preferred_element_type=f32
        )
    for e in range(devices):
        send_back[e] = big[e * items : (e + 1) * items, :].astype(bf16)

    exchange(send_back, back, send_back_sem, recv_back_sem, lambda: None)

    left = lax.broadcasted_iota(jnp.int32, (items, width), 1) < items
    for s in range(seqs):
        for g in range(groups):
            slot = (s * groups + g) * 2
            first, second = back[slot].astype(f32), back[slot + 1].astype(f32)
            halves = (
                jnp.where(left, first, pltpu.roll(second, items, 1)),
                jnp.where(left, pltpu.roll(first, items, 1), second),
            )
            for h in range(2):
                packed = jnp.dot(
                    halves[h].astype(bf16), maps[g], preferred_element_type=f32
                ).astype(bf16)
                for m in range(items // pairs):
                    base = m * devices + h * pairs
                    out_ref[s, base : base + pairs, g * width : (g + 1) * width] = packed[
                        m * pairs : (m + 1) * pairs
                    ]


def fused_lanes(mix_input, group_maps, pack, unpack, devices, scale):
    bf16, f32 = jnp.bfloat16, jnp.float32
    seqs, positions, channels = mix_input.shape
    width = pack.shape[0]
    items = seqs * channels // devices
    length = devices * positions
    twist_cos, twist_sin = turn_tables(devices, positions, length)
    pos_cos, pos_sin = turn_tables(positions, positions, positions)
    table = np.concatenate([pos_cos, pos_sin], axis=1) * scale
    slots = (devices, items, positions)
    vmem = pl.BlockSpec(memory_space=pltpu.VMEM)
    hbm = pl.BlockSpec(memory_space=pltpu.HBM)
    dma = pltpu.SemaphoreType.DMA((devices,))
    return pl.pallas_call(
        mixing_kernel,
        out_shape=jax.ShapeDtypeStruct(mix_input.shape, bf16),
        in_specs=[hbm] * 7,
        out_specs=vmem,
        scratch_shapes=[
            pltpu.VMEM(mix_input.shape, bf16), pltpu.VMEM(pack.shape, bf16),
            pltpu.VMEM(twist_cos.shape, f32), pltpu.VMEM(twist_sin.shape, f32),
            pltpu.VMEM(table.shape, bf16), pltpu.VMEM(unpack.shape, bf16),
            pltpu.VMEM(group_maps.shape, bf16), pltpu.VMEM(group_maps.shape, bf16),
            pltpu.SemaphoreType.DMA((7,)),
            pltpu.VMEM(slots, bf16), pltpu.VMEM(slots, bf16),
            pltpu.VMEM((devices, items, 2 * positions), bf16),
            pltpu.VMEM((devices * items, width), f32),
            pltpu.VMEM(slots, bf16), pltpu.VMEM(slots, bf16),
            dma, dma, dma, dma,
        ],
        compiler_params=pltpu.CompilerParams(
            collective_id=0, has_side_effects=True
        ),
    )(
        mix_input, jnp.asarray(pack.T, bf16), jnp.asarray(twist_cos, f32),
        jnp.asarray(twist_sin, f32), jnp.asarray(table, bf16), jnp.asarray(unpack, bf16), group_maps,
    )


def exchanged_lanes(mix_input, pack, width, devices, me, scale):
    bf16, f32 = jnp.bfloat16, jnp.float32
    seqs, positions, channels = mix_input.shape
    groups = channels // width
    length = devices * positions
    items = seqs * channels // devices
    lanes = jnp.einsum(
        "spgj,jc->sgcp",
        mix_input.reshape(seqs, positions, groups, width),
        jnp.asarray(pack, bf16),
        preferred_element_type=f32,
    ).astype(bf16)
    sent = lanes.reshape(devices, items, positions)
    held = lax.all_to_all(sent, AXES, split_axis=0, concat_axis=0, tiled=True)

    dev_cos, dev_sin = turn_tables(devices, devices, devices)
    both = jnp.asarray(np.concatenate([dev_cos, -dev_sin], axis=1), bf16)
    spun = jnp.einsum("df,dnp->fnp", both, held, preferred_element_type=f32)
    real_in, imag_in = spun[:devices], spun[devices:]
    twist_cos, twist_sin = turn_tables(devices, positions, length)
    twist_cos = jnp.asarray(twist_cos, f32)[:, None, :]
    twist_sin = jnp.asarray(twist_sin, f32)[:, None, :]
    real_part = real_in * twist_cos + imag_in * twist_sin
    imag_part = imag_in * twist_cos - real_in * twist_sin
    lane_ids = (me * items + jnp.arange(items, dtype=jnp.int32)) % width
    is_sine = ((lane_ids % 2 == 1) & (lane_ids != 1))[None, :, None]
    first = jnp.where(is_sine, -imag_part, real_part).astype(bf16)
    second = jnp.where(is_sine, real_part, imag_part).astype(bf16)
    stacked = jnp.concatenate([first, second], axis=2)
    pos_cos, pos_sin = turn_tables(positions, positions, positions)
    pos_table = jnp.asarray(np.concatenate([pos_cos, pos_sin], axis=0) * scale, bf16)
    freqs = jnp.einsum("pm,fnp->mfn", pos_table, stacked, preferred_element_type=f32).astype(bf16)

    freqs = freqs.reshape(devices, positions, items)
    back = lax.all_to_all(freqs, AXES, split_axis=0, concat_axis=0, tiled=True)
    parts = width // items
    back = back.reshape(seqs, groups, parts, positions, items)
    return back.transpose(0, 3, 1, 2, 4).reshape(seqs * positions, groups, width)


def per_device(mix_input, group_maps, out_map):
    bf16, f32 = jnp.bfloat16, jnp.float32
    seqs, positions, channels = mix_input.shape
    groups, width, _ = group_maps.shape
    devices = lax.axis_size("row") * lax.axis_size("col")
    me = lax.axis_index("row") * lax.axis_size("col") + lax.axis_index("col")
    items = seqs * channels // devices
    pack, unpack = lane_tables(width)
    scale = 1.0 / math.sqrt(devices * positions * width)
    if 2 * items == width and positions == width and items == 2 * devices:
        grouped = fused_lanes(mix_input, group_maps, pack, unpack, devices, scale)
    else:
        back = exchanged_lanes(mix_input, pack, width, devices, me, scale)
        maps = jnp.einsum(
            "cl,glm->gcm", jnp.asarray(unpack, bf16), group_maps, preferred_element_type=f32
        ).astype(bf16)
        grouped = jnp.einsum("rgc,gcm->rgm", back, maps, preferred_element_type=f32).astype(bf16)
    mixed = jnp.dot(
        grouped.reshape(seqs * positions, channels), out_map, preferred_element_type=f32
    )
    return mixed.astype(bf16).reshape(seqs, positions, out_map.shape[1])


def solution(mesh):
    return jax.shard_map(
        per_device,
        mesh=mesh,
        in_specs=(P(None, AXES, None), P(), P()),
        out_specs=P(None, AXES, None),
        check_vma=False,
    )
```

profile of v0, /device:TPU:0, one launch (start us, length us, event | category | flops | bytes accessed | tf_op | source)
XLA Modules:
  0.0 40.8 jit_solution(16398621087362191236)
XLA Ops:
  0.0 0.0 copy-start
  0.0 37.2 %shard_map.82 = bf16[4,128,512]{2,1,0:T(8,128)(2,1)} custom-call(bf16[4,128,512]{2,1,0:T(8,128)(2,1)} %x_hbm.1, bf16[128,128]{1,0:T(8,128)(2,1)} %constant.10.clone.pack_hbm, f32[32,128]{1,0:T(8,128)} %constant.11.clone.cos_hbm, f32[32,128]{1,0:T(8,128)} %constant.12.clone.sin_hbm, bf16[128,256]{1,0:T(8,128)(2,1)} %constant.13.clone.table_hbm, ...), custom_call_target="tpu_custom_call" | custom-call | tf_op jit(solution)/shard_map/pallas_call | solution.py:220
  37.2 0.0 copy-done
  37.2 3.6 %convolution_convert_fusion = bf16[512,2048]{1,0:T(8,128)(2,1)} fusion(bf16[512,512]{1,0:T(8,128)(2,1)} %bitcast.4, bf16[512,2048]{1,0:T(8,128)(2,1)S(1)} %copy-done), kind=kOutput, calls=%fused_computation | convolution fusion | flops 1074790400 | bytes 4718592 | tf_op jit(solution)/shard_map/dot_general | solution.py:303
Async XLA Ops:
  0.0 37.2 %copy-start = (bf16[512,2048]{1,0:T(8,128)(2,1)S(1)}, bf16[512,2048]{1,0:T(8,128)(2,1)}, u32[]{:S(2)}) copy-start(bf16[512,2048]{1,0:T(8,128)(2,1)} %param.10) | copy-start | bytes 6291460
where the time goes:
time: 41 us; the launch traced here: 40.8 us
  Pallas kernels  37.2 us (91%)
  matrix products  3.62 us (9%)
    pallas_call x1, Pallas kernels, fused_lanes(): pl.pallas_call(mixing_kernel, out_shape=jax.ShapeDtypeStruct(mix_input.sh...  37.2 us
    dot_general x1, matrix products, per_device(): jnp.dot(grouped.reshape(seqs * positions, channels), out_map, preferred_e...  3.62 us

commit v1 on v0

--- a/solution.py
+++ b/solution.py
@@ -69,9 +69,9 @@
 
 
 def mixing_kernel(
-    x_hbm, pack_hbm, cos_hbm, sin_hbm, table_hbm, unpack_hbm, given_hbm, out_ref,
-    x_ref, pack_ref, cos_ref, sin_ref, table_ref, unpack_ref, given_ref, maps, load_sem,
-    send, held, stack, big, send_back, back, send_sem, recv_sem, send_back_sem, recv_back_sem,
+    x_hbm, pack_hbm, cos_hbm, sin_hbm, table_hbm, unpack_hbm, given_hbm, outs_hbm, out_ref,
+    x_ref, pack_ref, cos_ref, sin_ref, table_ref, unpack_ref, given_ref, outs_ref, weights, load_sem,
+    send, held, stack, big, send_back, back, near, send_sem, recv_sem, send_back_sem, recv_back_sem,
 ):
     bf16, f32 = jnp.bfloat16, jnp.float32
     seqs, positions, channels = x_ref.shape
@@ -79,32 +79,59 @@
     width = pack_ref.shape[0]
     groups = channels // width
     cols = lax.axis_size("col")
-    me = lax.axis_index("row") * cols + lax.axis_index("col")
-    far_refs = (x_hbm, pack_hbm, cos_hbm, sin_hbm, table_hbm, unpack_hbm, given_hbm)
-    near_refs = (x_ref, pack_ref, cos_ref, sin_ref, table_ref, unpack_ref, given_ref)
+    row, col = lax.axis_index("row"), lax.axis_index("col")
+    me = row * cols + col
+    mesh_ids = pl.DeviceIdType.MESH
+    my_x, my_y = lax.rem(row, 2), lax.div(row, 2)
+    my_core, my_low, my_high = lax.rem(col, 2), lax.rem(lax.div(col, 2), 2), lax.div(col, 4)
+    members = devices // seqs
+    my_seq = 2 * my_core + lax.rem(my_x + my_y + my_low, 2)
+    my_slot = my_seq * members + row * 2 + my_high
+
+    far_refs = (pack_hbm, unpack_hbm, given_hbm, outs_hbm, cos_hbm, sin_hbm, table_hbm)
+    near_refs = (pack_ref, unpack_ref, given_ref, outs_ref, cos_ref, sin_ref, table_ref)
+    x_loads = [
+        pltpu.make_async_copy(x_hbm.at[s], x_ref.at[s], load_sem.at[s]) for s in range(seqs)
+    ]
     loads = [
-        pltpu.make_async_copy(src, dst, load_sem.at[at])
+        pltpu.make_async_copy(src, dst, load_sem.at[seqs + at])
         for at, (src, dst) in enumerate(zip(far_refs, near_refs))
     ]
-    for load in loads:
+    x_loads[0].start()
+    for load in (loads[0], *x_loads[1:], *loads[1:]):
         load.start()
     barrier = pltpu.get_barrier_semaphore()
 
-    def peer_of(step):
-        peer = lax.rem(me + step, devices)
-        return peer, (lax.div(peer, cols), lax.rem(peer, cols))
+    def turned(step):
+        x = lax.rem(my_x + lax.rem(step, 2), 2)
+        y = lax.rem(my_y + lax.rem(lax.div(step, 2), 2), 2)
+        core = lax.rem(my_core + lax.rem(lax.div(step, 4), 2), 2)
+        low = lax.rem(my_low + lax.rem(lax.div(step, 8), 2), 2)
+        high = lax.rem(my_high + lax.div(step, 16), 2)
+        return y * 2 + x, high * 4 + low * 2 + core
 
     def greet(step, carry):
         pl.semaphore_signal(
-            barrier, inc=1, device_id=peer_of(step)[1], device_id_type=pl.DeviceIdType.MESH
+            barrier, inc=1, device_id=turned(devices - step), device_id_type=mesh_ids
         )
         return carry
 
     lax.fori_loop(1, devices, greet, 0)
     rows_t = (((1,), (1,)), ((), ()))
-    loads[0].wait()
-    loads[1].wait()
+
+    def slot_copy(src, src_at, dst, dst_at, out_sem, in_sem, where):
+        return pltpu.make_async_remote_copy(
+            src_ref=src.at[src_at], dst_ref=dst.at[dst_at], send_sem=out_sem, recv_sem=in_sem,
+            device_id=where, device_id_type=mesh_ids,
+        )
+
+    def several(src, dst, count, out_sem, in_sem):
+        return slot_copy(src, pl.ds(0, count), dst, pl.ds(0, count), out_sem, in_sem, (row, col))
+
     for s in range(seqs):
+        x_loads[s].wait()
+        if s == 0:
+            loads[0].wait()
         for g in range(groups):
             lanes = lax.dot_general(
                 pack_ref[...], x_ref[s, :, g * width : (g + 1) * width], rows_t,
@@ -112,53 +139,41 @@
             ).astype(bf16)
             for half in range(2):
                 send[(s * groups + g) * 2 + half] = lanes[half * items : (half + 1) * items]
-    pl.semaphore_wait(barrier, devices - 1)
-
-    def exchange(src, dst, out_sem, in_sem, beside):
-        def copy(step):
-            peer, where = peer_of(step)
-            return pltpu.make_async_remote_copy(
-                src_ref=src.at[peer], dst_ref=dst.at[me], send_sem=out_sem.at[peer],
-                recv_sem=in_sem.at[me], device_id=where, device_id_type=pl.DeviceIdType.MESH,
-            )
-
-        def arrival(step):
-            peer, where = peer_of(step)
-            return pltpu.make_async_remote_copy(
-                src_ref=src.at[peer], dst_ref=dst.at[peer], send_sem=out_sem.at[peer],
-                recv_sem=in_sem.at[peer], device_id=where, device_id_type=pl.DeviceIdType.MESH,
-            )
+        if s == 0:
+            pl.semaphore_wait(barrier, devices - 1)
 
         def start(step, carry):
-            copy(step).start()
+            x = lax.rem(my_x + lax.rem(step, 2), 2)
+            y = lax.rem(my_y + lax.rem(lax.div(step, 2), 2), 2)
+            high = lax.rem(my_high + lax.div(step, 4), 2)
+            low = lax.rem(s % 2 + x + y, 2)
+            to_row, to_col = y * 2 + x, high * 4 + low * 2 + s // 2
+            slot_copy(
+                send, s * members + to_row * 2 + high, held, me, send_sem, recv_sem, (to_row, to_col)
+            ).start()
             return carry
 
-        def finish(step, carry):
-            arrival(step).wait_recv()
-            copy(step).wait_send()
-            return carry
-
-        lax.fori_loop(1, devices, start, 0)
-        dst[me] = src[me]
-        beside()
-        lax.fori_loop(1, devices, finish, 0)
-
-    def ready_maps():
-        for load in loads[2:]:
-            load.wait()
-        for g in range(groups):
-            maps[g] = jnp.dot(
-                unpack_ref[...], given_ref[g], preferred_element_type=f32
-            ).astype(bf16)
-
-    exchange(send, held, send_sem, recv_sem, ready_maps)
+        lax.fori_loop(jnp.where(my_seq == s, 1, 0), members, start, 0)
+    held[me] = send[my_slot]
+
+    for load in loads[1:4]:
+        load.wait()
+    for g in range(groups):
+        rows = slice(g * width, (g + 1) * width)
+        maps = jnp.dot(unpack_ref[...], given_ref[g], preferred_element_type=f32).astype(bf16)
+        weights[rows, :] = jnp.dot(
+            maps, outs_ref[rows, :], preferred_element_type=f32
+        ).astype(bf16)
+    for load in loads[4:]:
+        load.wait()
+    several(send, held, devices - 1, send_sem, recv_sem).wait_recv()
 
     tile = 16
     def spin(chunk, carry):
         rows = pl.ds(pl.multiple_of(chunk * tile, tile), tile)
         spun = fourier([(held[d, rows, :].astype(f32), None) for d in range(devices)])
         row_ids = chunk * tile + lax.broadcasted_iota(jnp.int32, (tile, positions), 0)
-        lane_ids = lax.rem(me * items + row_ids, width)
+        lane_ids = lax.rem(my_slot * items + row_ids, width)
         is_sine = (lax.rem(lane_ids, 2) == 1) & (lane_ids != 1)
         for f in range(devices):
             real_in, imag_in = spun[f]
@@ -182,29 +197,51 @@
     for e in range(devices):
         send_back[e] = big[e * items : (e + 1) * items, :].astype(bf16)
 
-    exchange(send_back, back, send_back_sem, recv_back_sem, lambda: None)
+    def start_back(step, carry):
+        to_row, to_col = turned(step)
+        slot_copy(
+            send_back, to_row * cols + to_col, back, my_slot, send_back_sem,
+            recv_back_sem.at[my_seq], (to_row, to_col),
+        ).start()
+        return carry
+
+    lax.fori_loop(1, devices, start_back, 0)
+    back[my_slot] = send_back[me]
+    several(send, held, devices - 1, send_sem, recv_sem).wait_send()
 
     left = lax.broadcasted_iota(jnp.int32, (items, width), 1) < items
-    for s in range(seqs):
+    chunk = 512
+
+    def finish(s, carry):
+        @pl.when(my_seq == s)
+        def _():
+            several(send_back, back, members - 1, send_back_sem, recv_back_sem.at[s]).wait_recv()
+
+        @pl.when(my_seq != s)
+        def _():
+            several(send_back, back, members, send_back_sem, recv_back_sem.at[s]).wait_recv()
+
         for g in range(groups):
-            slot = (s * groups + g) * 2
+            slot = s * members + g * 2
             first, second = back[slot].astype(f32), back[slot + 1].astype(f32)
-            halves = (
-                jnp.where(left, first, pltpu.roll(second, items, 1)),
-                jnp.where(left, pltpu.roll(first, items, 1), second),
-            )
+            lanes = slice(g * width, (g + 1) * width)
+            near[:items, lanes] = jnp.where(left, first, pltpu.roll(second, items, 1)).astype(bf16)
+            near[items:, lanes] = jnp.where(left, pltpu.roll(first, items, 1), second).astype(bf16)
+        for at in range(0, weights.shape[1], chunk):
+            made = jnp.dot(
+                near[...], weights[:, at : at + chunk], preferred_element_type=f32
+            ).astype(bf16)
             for h in range(2):
-                packed = jnp.dot(
-                    halves[h].astype(bf16), maps[g], preferred_element_type=f32
-                ).astype(bf16)
                 for m in range(items // pairs):
-                    base = m * devices + h * pairs
-                    out_ref[s, base : base + pairs, g * width : (g + 1) * width] = packed[
-                        m * pairs : (m + 1) * pairs
-                    ]
-
-
-def fused_lanes(mix_input, group_maps, pack, unpack, devices, scale):
+                    base, had = m * devices + h * pairs, h * items + m * pairs
+                    out_ref[s, base : base + pairs, at : at + chunk] = made[had : had + pairs]
+        return carry
+
+    lax.fori_loop(0, seqs, finish, 0)
+    several(send_back, back, devices - 1, send_back_sem, recv_back_sem.at[0]).wait_send()
+
+
+def fused_lanes(mix_input, group_maps, out_map, pack, unpack, devices, scale):
     bf16, f32 = jnp.bfloat16, jnp.float32
     seqs, positions, channels = mix_input.shape
     width = pack.shape[0]
@@ -214,25 +251,25 @@
     pos_cos, pos_sin = turn_tables(positions, positions, positions)
     table = np.concatenate([pos_cos, pos_sin], axis=1) * scale
     slots = (devices, items, positions)
-    vmem = pl.BlockSpec(memory_space=pltpu.VMEM)
     hbm = pl.BlockSpec(memory_space=pltpu.HBM)
-    dma = pltpu.SemaphoreType.DMA((devices,))
+    dma = pltpu.SemaphoreType.DMA
     return pl.pallas_call(
         mixing_kernel,
-        out_shape=jax.ShapeDtypeStruct(mix_input.shape, bf16),
-        in_specs=[hbm] * 7,
-        out_specs=vmem,
+        out_shape=pltpu.VMEM((seqs, positions, out_map.shape[1]), bf16),
+        in_specs=[hbm] * 8,
+        out_specs=pl.BlockSpec(memory_space=pltpu.VMEM),
         scratch_shapes=[
             pltpu.VMEM(mix_input.shape, bf16), pltpu.VMEM(pack.shape, bf16),
             pltpu.VMEM(twist_cos.shape, f32), pltpu.VMEM(twist_sin.shape, f32),
             pltpu.VMEM(table.shape, bf16), pltpu.VMEM(unpack.shape, bf16),
-            pltpu.VMEM(group_maps.shape, bf16), pltpu.VMEM(group_maps.shape, bf16),
-            pltpu.SemaphoreType.DMA((7,)),
+            pltpu.VMEM(group_maps.shape, bf16), pltpu.VMEM(out_map.shape, bf16),
+            pltpu.VMEM(out_map.shape, bf16), dma((seqs + 7,)),
             pltpu.VMEM(slots, bf16), pltpu.VMEM(slots, bf16),
             pltpu.VMEM((devices, items, 2 * positions), bf16),
             pltpu.VMEM((devices * items, width), f32),
             pltpu.VMEM(slots, bf16), pltpu.VMEM(slots, bf16),
-            dma, dma, dma, dma,
+            pltpu.VMEM((2 * items, channels), bf16),
+            dma, dma, dma, dma((seqs,)),
         ],
         compiler_params=pltpu.CompilerParams(
             collective_id=0, has_side_effects=True
@@ -240,6 +277,7 @@
     )(
         mix_input, jnp.asarray(pack.T, bf16), jnp.asarray(twist_cos, f32),
         jnp.asarray(twist_sin, f32), jnp.asarray(table, bf16), jnp.asarray(unpack, bf16), group_maps,
+        out_map,
     )
 
 
@@ -292,14 +330,14 @@
     items = seqs * channels // devices
     pack, unpack = lane_tables(width)
     scale = 1.0 / math.sqrt(devices * positions * width)
-    if 2 * items == width and positions == width and items == 2 * devices:
-        grouped = fused_lanes(mix_input, group_maps, pack, unpack, devices, scale)
-    else:
-        back = exchanged_lanes(mix_input, pack, width, devices, me, scale)
-        maps = jnp.einsum(
-            "cl,glm->gcm", jnp.asarray(unpack, bf16), group_maps, preferred_element_type=f32
-        ).astype(bf16)
-        grouped = jnp.einsum("rgc,gcm->rgm", back, maps, preferred_element_type=f32).astype(bf16)
+    square = 2 * items == width and positions == width and items == 2 * devices
+    if square and lax.axis_size("col") == 8 and seqs == 4:
+        return fused_lanes(mix_input, group_maps, out_map, pack, unpack, devices, scale)
+    back = exchanged_lanes(mix_input, pack, width, devices, me, scale)
+    maps = jnp.einsum(
+        "cl,glm->gcm", jnp.asarray(unpack, bf16), group_maps, preferred_element_type=f32
+    ).astype(bf16)
+    grouped = jnp.einsum("rgc,gcm->rgm", back, maps, preferred_element_type=f32).astype(bf16)
     mixed = jnp.dot(
         grouped.reshape(seqs * positions, channels), out_map, preferred_element_type=f32
     )

time: 41 us -> 36 us (0.88)
  matrix products: 3.62 us -> 0 us
  Pallas kernels: 37.2 us -> 34.6 us
  local copies, waits for them, and re-layouts: 0.01 us -> 1.32 us
    dot_general x1 -> x0, matrix products: 3.62 us -> none  [per_device(): jnp.dot(grouped.reshape(seqs * positions, channels), out_map, preferred_e...]
    pallas_call x1, Pallas kernels: 37.2 us -> 34.6 us  [fused_lanes(): pl.pallas_call(mixing_kernel, out_shape=pltpu.VMEM((seqs, positions, out_...]
    unnamed x2 -> x1, local copies, waits for them, and re-layouts: 0.01 us -> 1.32 us
where the time goes in v1:
time: 36 us; the launch traced here: 35.9 us
  Pallas kernels  34.6 us (96%)
  local copies, waits for them, and re-layouts  1.32 us (4%)
    pallas_call x1, Pallas kernels, fused_lanes(): pl.pallas_call(mixing_kernel, out_shape=pltpu.VMEM((seqs, positions, out_...  34.6 us
    unnamed x1, local copies, waits for them, and re-layouts  1.32 us

profile of v1, /device:TPU:0, one launch (start us, length us, event | category | flops | bytes accessed | tf_op | source)
XLA Modules:
  0.0 35.9 jit_solution(2495168353084197046)
XLA Ops:
  0.0 34.6 %shard_map.82 = bf16[4,128,2048]{2,1,0:T(8,128)(2,1)S(1)} custom-call(bf16[4,128,512]{2,1,0:T(8,128)(2,1)} %x_hbm.1, bf16[128,128]{1,0:T(8,128)(2,1)} %constant.10.clone.pack_hbm, f32[32,128]{1,0:T(8,128)} %constant.11.clone.cos_hbm, f32[32,128]{1,0:T(8,128)} %constant.12.clone.sin_hbm, bf16[128,256]{1,0:T(8,128)(2,1)} %constant.13.clone.table_hbm, ...), custom_call_target="tpu_custom_call" | custom-call | tf_op jit(solution)/shard_map/pallas_call | solution.py:256
  34.6 1.3 %copy.10 = bf16[4,128,2048]{2,1,0:T(8,128)(2,1)} copy(bf16[4,128,2048]{2,1,0:T(8,128)(2,1)S(1)} %shard_map.82) | data formatting | bytes 4194304

commit v2 on v1

--- a/solution.py
+++ b/solution.py
@@ -1,3 +1,4 @@
+import functools
 import math
 
 import jax
@@ -69,9 +70,10 @@
 
 
 def mixing_kernel(
-    x_hbm, pack_hbm, cos_hbm, sin_hbm, table_hbm, unpack_hbm, given_hbm, outs_hbm, out_ref,
-    x_ref, pack_ref, cos_ref, sin_ref, table_ref, unpack_ref, given_ref, outs_ref, weights, load_sem,
-    send, held, stack, big, send_back, back, near, send_sem, recv_sem, send_back_sem, recv_back_sem,
+    x_hbm, pack_hbm, cos_hbm, sin_hbm, table_hbm, unpack_hbm, given_hbm, outs_hbm,
+    out_ref, near, weights,
+    x_ref, pack_ref, cos_ref, sin_ref, table_ref, unpack_ref, given_ref, outs_ref, load_sem,
+    send, held, stack, big, send_back, back, send_sem, recv_sem, send_back_sem, recv_back_sem,
 ):
     bf16, f32 = jnp.bfloat16, jnp.float32
     seqs, positions, channels = x_ref.shape
@@ -82,41 +84,45 @@
     row, col = lax.axis_index("row"), lax.axis_index("col")
     me = row * cols + col
     mesh_ids = pl.DeviceIdType.MESH
-    my_x, my_y = lax.rem(row, 2), lax.div(row, 2)
-    my_core, my_low, my_high = lax.rem(col, 2), lax.rem(lax.div(col, 2), 2), lax.div(col, 4)
+    my_y, my_core, my_high = lax.div(row, 2), lax.rem(col, 2), lax.div(col, 4)
+    my_x = row - 2 * my_y
+    my_low = lax.div(col, 2) - 2 * my_high
+    my_inner = my_low + my_high - 2 * my_low * my_high
     members = devices // seqs
-    my_seq = 2 * my_core + lax.rem(my_x + my_y + my_low, 2)
-    my_slot = my_seq * members + row * 2 + my_high
+
+    def other(bit, turn):
+        return 1 - bit if turn else bit
+
+    def place(x, y, core, low, high):
+        inner = low + high - 2 * low * high
+        to_row, to_col = y * 2 + x, high * 4 + low * 2 + core
+        slot = (2 * core + lax.rem(x + y + low, 2)) * members + to_row * 2 + high
+        return to_row, to_col, slot
+
+    my_slot = place(my_x, my_y, my_core, my_low, my_high)[2]
+    my_seq = lax.div(my_slot, members)
 
     far_refs = (pack_hbm, unpack_hbm, given_hbm, outs_hbm, cos_hbm, sin_hbm, table_hbm)
-    near_refs = (pack_ref, unpack_ref, given_ref, outs_ref, cos_ref, sin_ref, table_ref)
+    local_refs = (pack_ref, unpack_ref, given_ref, outs_ref, cos_ref, sin_ref, table_ref)
     x_loads = [
         pltpu.make_async_copy(x_hbm.at[s], x_ref.at[s], load_sem.at[s]) for s in range(seqs)
     ]
     loads = [
         pltpu.make_async_copy(src, dst, load_sem.at[seqs + at])
-        for at, (src, dst) in enumerate(zip(far_refs, near_refs))
+        for at, (src, dst) in enumerate(zip(far_refs, local_refs))
     ]
-    x_loads[0].start()
-    for load in (loads[0], *x_loads[1:], *loads[1:]):
+    for load in (x_loads[0], loads[0], *x_loads[1:], *loads[1:]):
         load.start()
     barrier = pltpu.get_barrier_semaphore()
 
     def turned(step):
-        x = lax.rem(my_x + lax.rem(step, 2), 2)
-        y = lax.rem(my_y + lax.rem(lax.div(step, 2), 2), 2)
-        core = lax.rem(my_core + lax.rem(lax.div(step, 4), 2), 2)
-        low = lax.rem(my_low + lax.rem(lax.div(step, 8), 2), 2)
-        high = lax.rem(my_high + lax.div(step, 16), 2)
-        return y * 2 + x, high * 4 + low * 2 + core
-
-    def greet(step, carry):
+        bits = [step >> at & 1 for at in range(5)]
+        return place(*map(other, (my_x, my_y, my_core, my_low, my_high), bits))
+
+    for step in range(1, devices):
         pl.semaphore_signal(
-            barrier, inc=1, device_id=turned(devices - step), device_id_type=mesh_ids
+            barrier, inc=1, device_id=turned(step)[:2], device_id_type=mesh_ids
         )
-        return carry
-
-    lax.fori_loop(1, devices, greet, 0)
     rows_t = (((1,), (1,)), ((), ()))
 
     def slot_copy(src, src_at, dst, dst_at, out_sem, in_sem, where):
@@ -128,10 +134,8 @@
     def several(src, dst, count, out_sem, in_sem):
         return slot_copy(src, pl.ds(0, count), dst, pl.ds(0, count), out_sem, in_sem, (row, col))
 
-    for s in range(seqs):
+    def ready(s):
         x_loads[s].wait()
-        if s == 0:
-            loads[0].wait()
         for g in range(groups):
             lanes = lax.dot_general(
                 pack_ref[...], x_ref[s, :, g * width : (g + 1) * width], rows_t,
@@ -139,21 +143,27 @@
             ).astype(bf16)
             for half in range(2):
                 send[(s * groups + g) * 2 + half] = lanes[half * items : (half + 1) * items]
+
+    def send_to(where):
+        to_row, to_col, slot = where
+        slot_copy(send, slot, held, me, send_sem, recv_sem, (to_row, to_col)).start()
+
+    loads[0].wait()
+    for s in range(seqs):
+        ready(s)
         if s == 0:
             pl.semaphore_wait(barrier, devices - 1)
-
-        def start(step, carry):
-            x = lax.rem(my_x + lax.rem(step, 2), 2)
-            y = lax.rem(my_y + lax.rem(lax.div(step, 2), 2), 2)
-            high = lax.rem(my_high + lax.div(step, 4), 2)
+        for step in range(members - 1, -1, -1):
+            x, y, high = (other(bit, step >> at & 1) for at, bit in enumerate((my_x, my_y, my_high)))
             low = lax.rem(s % 2 + x + y, 2)
-            to_row, to_col = y * 2 + x, high * 4 + low * 2 + s // 2
-            slot_copy(
-                send, s * members + to_row * 2 + high, held, me, send_sem, recv_sem, (to_row, to_col)
-            ).start()
-            return carry
-
-        lax.fori_loop(jnp.where(my_seq == s, 1, 0), members, start, 0)
+            where = place(x, y, s // 2, low, high)
+            if step == 0:
+                @pl.when(my_seq != s)
+                def _():
+                    send_to(where)
+            else:
+                send_to(where)
+
     held[me] = send[my_slot]
 
     for load in loads[1:4]:
@@ -197,22 +207,18 @@
     for e in range(devices):
         send_back[e] = big[e * items : (e + 1) * items, :].astype(bf16)
 
-    def start_back(step, carry):
-        to_row, to_col = turned(step)
+    for step in range(1, devices):
+        to_row, to_col, _ = turned(step)
         slot_copy(
             send_back, to_row * cols + to_col, back, my_slot, send_back_sem,
             recv_back_sem.at[my_seq], (to_row, to_col),
         ).start()
-        return carry
-
-    lax.fori_loop(1, devices, start_back, 0)
     back[my_slot] = send_back[me]
     several(send, held, devices - 1, send_sem, recv_sem).wait_send()
 
     left = lax.broadcasted_iota(jnp.int32, (items, width), 1) < items
-    chunk = 512
-
-    def finish(s, carry):
+
+    def gather(s):
         @pl.when(my_seq == s)
         def _():
             several(send_back, back, members - 1, send_back_sem, recv_back_sem.at[s]).wait_recv()
@@ -227,18 +233,55 @@
             lanes = slice(g * width, (g + 1) * width)
             near[:items, lanes] = jnp.where(left, first, pltpu.roll(second, items, 1)).astype(bf16)
             near[items:, lanes] = jnp.where(left, pltpu.roll(first, items, 1), second).astype(bf16)
-        for at in range(0, weights.shape[1], chunk):
-            made = jnp.dot(
-                near[...], weights[:, at : at + chunk], preferred_element_type=f32
-            ).astype(bf16)
-            for h in range(2):
-                for m in range(items // pairs):
-                    base, had = m * devices + h * pairs, h * items + m * pairs
-                    out_ref[s, base : base + pairs, at : at + chunk] = made[had : had + pairs]
+
+    def finish(s, carry):
+        gather(s)
+        product(near, weights, out_ref.at[s], devices)
         return carry
 
-    lax.fori_loop(0, seqs, finish, 0)
+    lax.fori_loop(0, seqs - 1, finish, 0)
+    gather(seqs - 1)
     several(send_back, back, devices - 1, send_back_sem, recv_back_sem.at[0]).wait_send()
+
+
+CHUNK = 512
+
+
+def product(near, weights, out_ref, devices, done=None):
+    positions = near.shape[0]
+    items, pairs = positions // 2, devices // 2
+    for at in range(0, weights.shape[1], CHUNK):
+        made = jnp.dot(
+            near[...], weights[:, at : at + CHUNK], preferred_element_type=jnp.float32
+        ).astype(jnp.bfloat16)
+        for h in range(2):
+            for m in range(items // pairs):
+                base, had = m * devices + h * pairs, h * items + m * pairs
+                out_ref[base : base + pairs, at : at + CHUNK] = made[had : had + pairs]
+        if done is not None:
+            done(at)
+
+
+def last_kernel(devices, early, near, weights, out_hbm, late, early_sem, late_sem):
+    seqs = early.shape[0] + 1
+    early_copies = [
+        pltpu.make_async_copy(early.at[s], out_hbm.at[s], early_sem.at[s]) for s in range(seqs - 1)
+    ]
+    for copy in early_copies:
+        copy.start()
+    late_copies = []
+
+    def done(at):
+        lanes = pl.ds(at, CHUNK)
+        copy = pltpu.make_async_copy(
+            late.at[:, lanes], out_hbm.at[seqs - 1, :, lanes], late_sem.at[at // CHUNK]
+        )
+        copy.start()
+        late_copies.append(copy)
+
+    product(near, weights, late, devices, done)
+    for copy in early_copies + late_copies:
+        copy.wait()
 
 
 def fused_lanes(mix_input, group_maps, out_map, pack, unpack, devices, scale):
@@ -253,32 +296,47 @@
     slots = (devices, items, positions)
     hbm = pl.BlockSpec(memory_space=pltpu.HBM)
     dma = pltpu.SemaphoreType.DMA
-    return pl.pallas_call(
+    vmem = pl.BlockSpec(memory_space=pltpu.VMEM)
+    model = out_map.shape[1]
+    given = (
+        mix_input, jnp.asarray(pack.T, bf16), jnp.asarray(twist_cos, f32),
+        jnp.asarray(twist_sin, f32), jnp.asarray(table, bf16), jnp.asarray(unpack, bf16), group_maps,
+        out_map,
+    )
+    early, near, weights = pl.pallas_call(
         mixing_kernel,
-        out_shape=pltpu.VMEM((seqs, positions, out_map.shape[1]), bf16),
+        out_shape=[
+            pltpu.VMEM((seqs - 1, positions, model), bf16), pltpu.VMEM((positions, channels), bf16),
+            pltpu.VMEM(out_map.shape, bf16),
+        ],
         in_specs=[hbm] * 8,
-        out_specs=pl.BlockSpec(memory_space=pltpu.VMEM),
+        out_specs=[vmem] * 3,
         scratch_shapes=[
             pltpu.VMEM(mix_input.shape, bf16), pltpu.VMEM(pack.shape, bf16),
             pltpu.VMEM(twist_cos.shape, f32), pltpu.VMEM(twist_sin.shape, f32),
             pltpu.VMEM(table.shape, bf16), pltpu.VMEM(unpack.shape, bf16),
-            pltpu.VMEM(group_maps.shape, bf16), pltpu.VMEM(out_map.shape, bf16),
-            pltpu.VMEM(out_map.shape, bf16), dma((seqs + 7,)),
+            pltpu.VMEM(group_maps.shape, bf16), pltpu.VMEM(out_map.shape, bf16), dma((seqs + 7,)),
             pltpu.VMEM(slots, bf16), pltpu.VMEM(slots, bf16),
             pltpu.VMEM((devices, items, 2 * positions), bf16),
             pltpu.VMEM((devices * items, width), f32),
             pltpu.VMEM(slots, bf16), pltpu.VMEM(slots, bf16),
-            pltpu.VMEM((2 * items, channels), bf16),
             dma, dma, dma, dma((seqs,)),
         ],
         compiler_params=pltpu.CompilerParams(
-            collective_id=0, has_side_effects=True
+            collective_id=0, has_side_effects=True, vmem_limit_bytes=32 << 20
         ),
-    )(
-        mix_input, jnp.asarray(pack.T, bf16), jnp.asarray(twist_cos, f32),
-        jnp.asarray(twist_sin, f32), jnp.asarray(table, bf16), jnp.asarray(unpack, bf16), group_maps,
-        out_map,
-    )
+    )(*(pltpu.with_memory_space_constraint(value, pltpu.HBM) for value in given))
+    kept = [pltpu.with_memory_space_constraint(value, pltpu.VMEM) for value in (early, near, weights)]
+    return pl.pallas_call(
+        functools.partial(last_kernel, devices),
+        out_shape=jax.ShapeDtypeStruct((seqs, positions, model), bf16),
+        in_specs=[vmem] * 3,
+        out_specs=hbm,
+        scratch_shapes=[
+            pltpu.VMEM((positions, model), bf16), dma((seqs - 1,)), dma((model // CHUNK,)),
+        ],
+        compiler_params=pltpu.CompilerParams(vmem_limit_bytes=16 << 20),
+    )(*kept)
 
 
 def exchanged_lanes(mix_input, pack, width, devices, me, scale):

time: 36 us -> 33.1 us (0.919)
  Pallas kernels: 34.6 us -> 33 us
  local copies, waits for them, and re-layouts: 1.32 us -> 0 us
    pallas_call x1 -> x2, Pallas kernels: 34.6 us -> 33 us  [the longest x1 31.6 us: fused_lanes(): pl.pallas_call(mixing_kernel, out_shape=[pltpu.VMEM((seqs - 1, positions,...]
    unnamed x1 -> x0, local copies, waits for them, and re-layouts: 1.32 us -> none
where the time goes in v2:
time: 33.1 us; the launch traced here: 33 us
  Pallas kernels  33 us (100%)
    pallas_call x1, Pallas kernels, fused_lanes(): pl.pallas_call(mixing_kernel, out_shape=[pltpu.VMEM((seqs - 1, positions,...  31.6 us
    pallas_call x1, Pallas kernels, fused_lanes(): pl.pallas_call(functools.partial(last_kernel, devices), out_shape=jax.Sha...  1.36 us

profile of v2, /device:TPU:0, one launch (start us, length us, event | category | flops | bytes accessed | tf_op | source)
XLA Modules:
  0.0 33.0 jit_solution(4724550095416115988)
XLA Ops:
  0.0 31.6 %shard_map.82 = (bf16[3,128,2048]{2,1,0:T(8,128)(2,1)S(1)}, bf16[128,512]{1,0:T(8,128)(2,1)S(1)}, bf16[512,2048]{1,0:T(8,128)(2,1)S(1)}) custom-call(bf16[4,128,512]{2,1,0:T(8,128)(2,1)} %x_hbm.1, bf16[128,128]{1,0:T(8,128)(2,1)} %constant.10.clone.pack_hbm, f32[32,128]{1,0:T(8,128)} %constant.11.clone.cos_hbm, f32[32,128]{1,0:T(8,128)} %constant.12.clone.sin_hbm, ...), custom_call_target="tpu_custom_call" | custom-call | tf_op jit(solution)/shard_map/pallas_call | solution.py:306
  31.6 1.4 %shard_map.83 = bf16[4,128,2048]{2,1,0:T(8,128)(2,1)} custom-call(bf16[3,128,2048]{2,1,0:T(8,128)(2,1)S(1)} %get-tuple-element.8.early, bf16[128,512]{1,0:T(8,128)(2,1)S(1)} %get-tuple-element.9.near, bf16[512,2048]{1,0:T(8,128)(2,1)S(1)} %get-tuple-element.10.weights), custom_call_target="tpu_custom_call" | custom-call | tf_op jit(solution)/shard_map/pallas_call | solution.py:330

commit v3 on v2

--- a/solution.py
+++ b/solution.py
@@ -38,35 +38,26 @@
 def fourier(values):
     count = len(values)
     if count == 1:
-        return values
+        return [(values[0], None)]
+    if count == 2:
+        return [(values[0] + values[1], None), (values[0] - values[1], None)]
     even, odd = fourier(values[0::2]), fourier(values[1::2])
     low, high = [], []
-    for at in range(count // 2):
-        cosine = math.cos(2.0 * math.pi * at / count)
-        sine = math.sin(2.0 * math.pi * at / count)
+    for at in range(count // 4 + 1):
         (even_re, even_im), (odd_re, odd_im) = even[at], odd[at]
         if at == 0:
-            turn_re, turn_im = odd_re, odd_im
+            low.append((even_re + odd_re, None))
+            high.append((even_re - odd_re, None))
         elif 4 * at == count:
-            turn_re, turn_im = odd_im, -odd_re
-        elif odd_im is None:
-            turn_re, turn_im = odd_re * cosine, odd_re * -sine
+            low.append((even_re, -odd_re))
         else:
+            cosine = math.cos(2.0 * math.pi * at / count)
+            sine = math.sin(2.0 * math.pi * at / count)
             turn_re = odd_re * cosine + odd_im * sine
             turn_im = odd_im * cosine - odd_re * sine
-        if turn_re is None:
-            low_re = high_re = even_re
-        else:
-            low_re, high_re = even_re + turn_re, even_re - turn_re
-        if turn_im is None:
-            low_im = high_im = even_im
-        elif even_im is None:
-            low_im, high_im = turn_im, -turn_im
-        else:
-            low_im, high_im = even_im + turn_im, even_im - turn_im
-        low.append((low_re, low_im))
-        high.append((high_re, high_im))
-    return low + high
+            low.append((even_re + turn_re, even_im + turn_im))
+            high.append((even_re - turn_re, turn_im - even_im))
+    return low + high[::-1]
 
 
 def mixing_kernel(
@@ -74,6 +65,7 @@
     out_ref, near, weights,
     x_ref, pack_ref, cos_ref, sin_ref, table_ref, unpack_ref, given_ref, outs_ref, load_sem,
     send, held, stack, big, send_back, back, send_sem, recv_sem, send_back_sem, recv_back_sem,
+    twist_a, twist_b,
 ):
     bf16, f32 = jnp.bfloat16, jnp.float32
     seqs, positions, channels = x_ref.shape
@@ -153,17 +145,17 @@
         ready(s)
         if s == 0:
             pl.semaphore_wait(barrier, devices - 1)
-        for step in range(members - 1, -1, -1):
-            x, y, high = (other(bit, step >> at & 1) for at, bit in enumerate((my_x, my_y, my_high)))
-            low = lax.rem(s % 2 + x + y, 2)
-            where = place(x, y, s // 2, low, high)
-            if step == 0:
-                @pl.when(my_seq != s)
+        for turn_high, outer, turn_x in ((1, 1, 1), (1, 1, 0), (1, 0, 1), (1, 0, 0), (0, 0, 1), (0, 0, 0), (0, 1, 1), (0, 1, 0)):
+            x, high = other(my_x, turn_x), other(my_high, turn_high)
+            kind = lax.rem(s + high + outer, 2)
+            y = x + kind - 2 * x * kind
+            where = place(x, y, s // 2, lax.rem(s % 2 + x + y, 2), high)
+            if turn_high or turn_x:
+                send_to(where)
+            else:
+                @pl.when(where[0] * cols + where[1] != me)
                 def _():
                     send_to(where)
-            else:
-                send_to(where)
-
     held[me] = send[my_slot]
 
     for load in loads[1:4]:
@@ -176,43 +168,68 @@
         ).astype(bf16)
     for load in loads[4:]:
         load.wait()
+    tile = twist_a.shape[2]
+    row_ids = lax.broadcasted_iota(jnp.int32, (tile, positions), 0)
+    for kind in range(2):
+        is_sine = lax.rem(row_ids, 2) == 1
+        if kind == 1:
+            is_sine = is_sine & (row_ids != 1)
+        for f in range(devices):
+            cosine, sine = cos_ref[f : f + 1, :], sin_ref[f : f + 1, :]
+            twist_a[kind, f] = jnp.where(is_sine, sine, cosine)
+            twist_b[kind, f] = jnp.where(is_sine, -cosine, sine)
     several(send, held, devices - 1, send_sem, recv_sem).wait_recv()
 
-    tile = 16
     def spin(chunk, carry):
         rows = pl.ds(pl.multiple_of(chunk * tile, tile), tile)
-        spun = fourier([(held[d, rows, :].astype(f32), None) for d in range(devices)])
-        row_ids = chunk * tile + lax.broadcasted_iota(jnp.int32, (tile, positions), 0)
-        lane_ids = lax.rem(my_slot * items + row_ids, width)
-        is_sine = (lax.rem(lane_ids, 2) == 1) & (lane_ids != 1)
+        kind = jnp.where((chunk == 0) & (lax.rem(my_slot, 2) == 0), 1, 0)
+        spun = fourier([held[d, rows, :].astype(f32) for d in range(devices)])
         for f in range(devices):
-            real_in, imag_in = spun[f]
-            cosine, sine = cos_ref[f : f + 1, :], sin_ref[f : f + 1, :]
-            if imag_in is None:
-                real_part, imag_part = real_in * cosine, -(real_in * sine)
+            real, imag = spun[min(f, devices - f)]
+            turn_a, turn_b = twist_a[kind, f], twist_b[kind, f]
+            if imag is None:
+                first, second = real * turn_a, -(real * turn_b)
+            elif 2 * f < devices:
+                first, second = real * turn_a + imag * turn_b, imag * turn_a - real * turn_b
             else:
-                real_part = real_in * cosine + imag_in * sine
-                imag_part = imag_in * cosine - real_in * sine
-            stack[f, rows, :positions] = jnp.where(is_sine, -imag_part, real_part).astype(bf16)
-            stack[f, rows, positions:] = jnp.where(is_sine, real_part, imag_part).astype(bf16)
+                first, second = real * turn_a - imag * turn_b, -(imag * turn_a + real * turn_b)
+            stack[f, rows, :positions] = first.astype(bf16)
+            stack[f, rows, positions:] = second.astype(bf16)
         return carry
 
     lax.fori_loop(0, items // tile, spin, 0)
     pairs = devices // 2
-    for a in range(pairs):
-        both = jnp.concatenate([stack[a], stack[a + pairs]], axis=0)
-        big[pl.ds(a, positions, stride=pairs), :] = lax.dot_general(
-            table_ref[...], both, rows_t, preferred_element_type=f32
+    for a in range(0, pairs, 2):
+        both = jnp.concatenate(
+            [stack[a], stack[a + pairs], stack[a + 1], stack[a + 1 + pairs]], axis=0
         )
+        made = lax.dot_general(table_ref[...], both, rows_t, preferred_element_type=f32)
+        big[pl.ds(a, positions, stride=pairs), :] = made[:, :width]
+        big[pl.ds(a + 1, positions, stride=pairs), :] = made[:, width:]
     for e in range(devices):
         send_back[e] = big[e * items : (e + 1) * items, :].astype(bf16)
 
-    for step in range(1, devices):
-        to_row, to_col, _ = turned(step)
-        slot_copy(
-            send_back, to_row * cols + to_col, back, my_slot, send_back_sem,
-            recv_back_sem.at[my_seq], (to_row, to_col),
-        ).start()
+    def back_to(where, first):
+        to_row, to_col, _ = where
+
+        def go():
+            slot_copy(
+                send_back, to_row * cols + to_col, back, my_slot, send_back_sem,
+                recv_back_sem.at[my_seq], (to_row, to_col),
+            ).start()
+
+        at = to_row * cols + to_col
+        if first:
+            pl.when(at != me)(go)
+        else:
+            pl.when((at != me) & (at >= 2))(go)
+
+    for core in range(2):
+        back_to((0, core, None), True)
+    for level, step, core in ((0, 3, 0), (0, 2, 0), (0, 3, 1), (0, 2, 1), (0, 1, 0), (0, 0, 0), (0, 1, 1), (0, 0, 1), (1, 3, 0), (1, 2, 0), (1, 3, 1), (1, 2, 1), (1, 1, 0), (1, 0, 0), (1, 1, 1), (1, 0, 1), (2, 3, 0), (2, 2, 0), (2, 3, 1), (2, 2, 1), (2, 1, 0), (2, 0, 0), (2, 1, 1), (2, 0, 1), (3, 3, 0), (3, 2, 0), (3, 3, 1), (3, 2, 1), (3, 1, 0), (3, 0, 0), (3, 1, 1), (3, 0, 1)):
+        x, y = other(my_x, step & 1), other(my_y, step >> 1)
+        back_to(place(x, y, core, level % 2, level // 2), False)
+
     back[my_slot] = send_back[me]
     several(send, held, devices - 1, send_sem, recv_sem).wait_send()
 
@@ -321,6 +338,7 @@
             pltpu.VMEM((devices * items, width), f32),
             pltpu.VMEM(slots, bf16), pltpu.VMEM(slots, bf16),
             dma, dma, dma, dma((seqs,)),
+            pltpu.VMEM((2, devices, 16, positions), f32), pltpu.VMEM((2, devices, 16, positions), f32),
         ],
         compiler_params=pltpu.CompilerParams(
             collective_id=0, has_side_effects=True, vmem_limit_bytes=32 << 20

time: 33.1 us -> 30.8 us (0.931)
  Pallas kernels: 33 us -> 30.6 us
    pallas_call x1, Pallas kernels: 31.6 us -> 29.2 us  [fused_lanes(): pl.pallas_call(mixing_kernel, out_shape=[pltpu.VMEM((seqs - 1, positions,...]
where the time goes in v3:
time: 30.8 us; the launch traced here: 30.6 us
  Pallas kernels  30.6 us (99%)
    pallas_call x1, Pallas kernels, fused_lanes(): pl.pallas_call(mixing_kernel, out_shape=[pltpu.VMEM((seqs - 1, positions,...  29.2 us
    pallas_call x1, Pallas kernels, fused_lanes(): pl.pallas_call(functools.partial(last_kernel, devices), out_shape=jax.Sha...  1.36 us

profile of v3, /device:TPU:0, one launch (start us, length us, event | category | flops | bytes accessed | tf_op | source)
XLA Modules:
  0.0 30.6 jit_solution(17204013972805432953)
XLA Ops:
  0.0 29.2 %shard_map.82 = (bf16[3,128,2048]{2,1,0:T(8,128)(2,1)S(1)}, bf16[128,512]{1,0:T(8,128)(2,1)S(1)}, bf16[512,2048]{1,0:T(8,128)(2,1)S(1)}) custom-call(bf16[4,128,512]{2,1,0:T(8,128)(2,1)} %x_hbm.1, bf16[128,128]{1,0:T(8,128)(2,1)} %constant.10.clone.pack_hbm, f32[32,128]{1,0:T(8,128)} %constant.11.clone.cos_hbm, f32[32,128]{1,0:T(8,128)} %constant.12.clone.sin_hbm, ...), custom_call_target="tpu_custom_call" | custom-call | tf_op jit(solution)/shard_map/pallas_call | solution.py:323
  29.2 1.4 %shard_map.83 = bf16[4,128,2048]{2,1,0:T(8,128)(2,1)} custom-call(bf16[3,128,2048]{2,1,0:T(8,128)(2,1)S(1)} %get-tuple-element.8.early, bf16[128,512]{1,0:T(8,128)(2,1)S(1)} %get-tuple-element.9.near, bf16[512,2048]{1,0:T(8,128)(2,1)S(1)} %get-tuple-element.10.weights), custom_call_target="tpu_custom_call" | custom-call | tf_op jit(solution)/shard_map/pallas_call | solution.py:348

commit v4 on v3

--- a/solution.py
+++ b/solution.py
@@ -65,7 +65,7 @@
     out_ref, near, weights,
     x_ref, pack_ref, cos_ref, sin_ref, table_ref, unpack_ref, given_ref, outs_ref, load_sem,
     send, held, stack, big, send_back, back, send_sem, recv_sem, send_back_sem, recv_back_sem,
-    twist_a, twist_b,
+    twist_a, twist_b, ends,
 ):
     bf16, f32 = jnp.bfloat16, jnp.float32
     seqs, positions, channels = x_ref.shape
@@ -111,10 +111,20 @@
         bits = [step >> at & 1 for at in range(5)]
         return place(*map(other, (my_x, my_y, my_core, my_low, my_high), bits))
 
-    for step in range(1, devices):
-        pl.semaphore_signal(
-            barrier, inc=1, device_id=turned(step)[:2], device_id_type=mesh_ids
-        )
+    def tell(sem, steps):
+        for step in steps:
+            pl.semaphore_signal(
+                sem, inc=1, device_id=turned(step)[:2], device_id_type=mesh_ids
+            )
+
+    same_kind = [step for step in range(1, devices) if step // 8 in (0, 3)]
+    other_kind = [step for step in range(1, devices) if step // 8 in (1, 2)]
+    tell(barrier, same_kind)
+
+    @pl.when(my_inner == 1)
+    def _():
+        tell(barrier, other_kind)
+
     rows_t = (((1,), (1,)), ((), ()))
 
     def slot_copy(src, src_at, dst, dst_at, out_sem, in_sem, where):
@@ -140,22 +150,58 @@
         to_row, to_col, slot = where
         slot_copy(send, slot, held, me, send_sem, recv_sem, (to_row, to_col)).start()
 
+    def first_of(s, turn_high, outer, turn_x):
+        x, high = other(my_x, turn_x), other(my_high, turn_high)
+        kind = lax.rem(s + high + outer, 2)
+        y = x + kind - 2 * x * kind
+        return place(x, y, s // 2, lax.rem(s % 2 + x + y, 2), high)
+
+    def send_but_me(where):
+        @pl.when(where[0] * cols + where[1] != me)
+        def _():
+            send_to(where)
+
+    def to_end(s, high):
+        for turn_x in (1, 0):
+            x = other(my_x, turn_x)
+            kind = (s + high) % 2
+            y = x + kind - 2 * x * kind
+            send_to(place(x, y, s // 2, high, high))
+
     loads[0].wait()
-    for s in range(seqs):
-        ready(s)
-        if s == 0:
-            pl.semaphore_wait(barrier, devices - 1)
-        for turn_high, outer, turn_x in ((1, 1, 1), (1, 1, 0), (1, 0, 1), (1, 0, 0), (0, 0, 1), (0, 0, 0), (0, 1, 1), (0, 1, 0)):
-            x, high = other(my_x, turn_x), other(my_high, turn_high)
-            kind = lax.rem(s + high + outer, 2)
-            y = x + kind - 2 * x * kind
-            where = place(x, y, s // 2, lax.rem(s % 2 + x + y, 2), high)
-            if turn_high or turn_x:
-                send_to(where)
-            else:
-                @pl.when(where[0] * cols + where[1] != me)
-                def _():
+
+    @pl.when(my_inner == 0)
+    def _():
+        for s in range(seqs):
+            ready(s)
+            if s == 0:
+                pl.semaphore_wait(barrier, devices - 1)
+                tell(ends.at[my_high], other_kind)
+            for turn_high, outer, turn_x in ((1, 1, 1), (1, 1, 0), (1, 0, 1), (1, 0, 0), (0, 0, 1), (0, 0, 0), (0, 1, 1), (0, 1, 0)):
+                where = first_of(s, turn_high, outer, turn_x)
+                if turn_high or turn_x:
                     send_to(where)
+                else:
+                    send_but_me(where)
+
+    @pl.when(my_inner == 1)
+    def _():
+        for s in range(seqs):
+            ready(s)
+        pl.semaphore_wait(barrier, devices // 2 - 1)
+        for s in range(seqs):
+            for turn_x in (1, 0):
+                send_to(first_of(s, 1, 1, turn_x))
+        pl.semaphore_wait(ends.at[1], devices // 4)
+        for s in range(seqs):
+            to_end(s, 1)
+        pl.semaphore_wait(ends.at[0], devices // 4)
+        for s in range(seqs):
+            to_end(s, 0)
+        for s in range(seqs):
+            send_to(first_of(s, 0, 1, 1))
+            send_but_me(first_of(s, 0, 1, 0))
+
     held[me] = send[my_slot]
 
     for load in loads[1:4]:
@@ -222,11 +268,11 @@
         if first:
             pl.when(at != me)(go)
         else:
-            pl.when((at != me) & (at >= 2))(go)
-
-    for core in range(2):
-        back_to((0, core, None), True)
-    for level, step, core in ((0, 3, 0), (0, 2, 0), (0, 3, 1), (0, 2, 1), (0, 1, 0), (0, 0, 0), (0, 1, 1), (0, 0, 1), (1, 3, 0), (1, 2, 0), (1, 3, 1), (1, 2, 1), (1, 1, 0), (1, 0, 0), (1, 1, 1), (1, 0, 1), (2, 3, 0), (2, 2, 0), (2, 3, 1), (2, 2, 1), (2, 1, 0), (2, 0, 0), (2, 1, 1), (2, 0, 1), (3, 3, 0), (3, 2, 0), (3, 3, 1), (3, 2, 1), (3, 1, 0), (3, 0, 0), (3, 1, 1), (3, 0, 1)):
+            pl.when((at != me) & (at >= 8))(go)
+
+    for to_col in range(8):
+        back_to((0, to_col, None), True)
+    for level, step, core in ((0, 3, 1), (0, 3, 0), (0, 2, 1), (0, 2, 0), (1, 3, 1), (0, 1, 1), (1, 3, 0), (0, 1, 0), (1, 2, 1), (0, 0, 1), (1, 2, 0), (0, 0, 0), (1, 1, 1), (1, 1, 0), (1, 0, 1), (1, 0, 0), (2, 3, 1), (2, 3, 0), (2, 2, 1), (2, 2, 0), (3, 3, 1), (2, 1, 1), (3, 3, 0), (2, 1, 0), (3, 2, 1), (2, 0, 1), (3, 2, 0), (2, 0, 0), (3, 1, 1), (3, 1, 0), (3, 0, 1), (3, 0, 0)):
         x, y = other(my_x, step & 1), other(my_y, step >> 1)
         back_to(place(x, y, core, level % 2, level // 2), False)
 
@@ -339,6 +385,7 @@
             pltpu.VMEM(slots, bf16), pltpu.VMEM(slots, bf16),
             dma, dma, dma, dma((seqs,)),
             pltpu.VMEM((2, devices, 16, positions), f32), pltpu.VMEM((2, devices, 16, positions), f32),
+            pltpu.SemaphoreType.REGULAR((2,)),
         ],
         compiler_params=pltpu.CompilerParams(
             collective_id=0, has_side_effects=True, vmem_limit_bytes=32 << 20

time: 30.8 us -> 30.8 us (level)
  the two profiles are of different devices: /device:TPU:0 before, /device:TPU:10 now
where the time goes in v4:
time: 30.8 us; the launch traced here: 30.7 us
  Pallas kernels  30.6 us (99%)
    pallas_call x1, Pallas kernels, fused_lanes(): pl.pallas_call(mixing_kernel, out_shape=[pltpu.VMEM((seqs - 1, positions,...  29.3 us
    pallas_call x1, Pallas kernels, fused_lanes(): pl.pallas_call(functools.partial(last_kernel, devices), out_shape=jax.Sha...  1.36 us

profile of v4, /device:TPU:10, one launch (start us, length us, event | category | flops | bytes accessed | tf_op | source)
XLA Modules:
  0.0 30.7 jit_solution(12423564282384416961)
XLA Ops:
  0.0 29.3 %shard_map.82 = (bf16[3,128,2048]{2,1,0:T(8,128)(2,1)S(1)}, bf16[128,512]{1,0:T(8,128)(2,1)S(1)}, bf16[512,2048]{1,0:T(8,128)(2,1)S(1)}) custom-call(bf16[4,128,512]{2,1,0:T(8,128)(2,1)} %x_hbm.1, bf16[128,128]{1,0:T(8,128)(2,1)} %constant.10.clone.pack_hbm, f32[32,128]{1,0:T(8,128)} %constant.11.clone.cos_hbm, f32[32,128]{1,0:T(8,128)} %constant.12.clone.sin_hbm, ...), custom_call_target="tpu_custom_call" | custom-call | tf_op jit(solution)/shard_map/pallas_call | solution.py:369
  29.3 1.4 %shard_map.83 = bf16[4,128,2048]{2,1,0:T(8,128)(2,1)} custom-call(bf16[3,128,2048]{2,1,0:T(8,128)(2,1)S(1)} %get-tuple-element.8.early, bf16[128,512]{1,0:T(8,128)(2,1)S(1)} %get-tuple-element.9.near, bf16[512,2048]{1,0:T(8,128)(2,1)S(1)} %get-tuple-element.10.weights), custom_call_target="tpu_custom_call" | custom-call | tf_op jit(solution)/shard_map/pallas_call | solution.py:395
